TPU v7x, 32 devices: a whole 2x2x4 slice. The times are simulated.
32 devices in a mesh: sp: 16 (over z, y, x), tp: 2 (over core).
Axes of the slice: x: 2, y: 2, z: 4, core: 2. Of those that a mesh axis runs over, the one named last changes fastest.
Arguments:
- residual_in: bfloat16 [8192, 2048], P(('sp', 'tp')), may hold values from -6 to 6
- queries: bfloat16 [8192, 2048], P('sp', 'tp'), may hold values from -200 to 200
- keys: bfloat16 [8192, 512], P('sp', 'tp'), may hold values from -5.5 to 5.5
- values: bfloat16 [8192, 512], P('sp', 'tp'), may hold values from -6 to 6
- docs: int32 [8192], P('sp'), may hold values from 0 to 3, never falling along the last dimension, each value on 1 to 4096 neighbouring positions
- sink: float32 [32], P('tp'), may hold values from 1 to 7
- out_weight: bfloat16 [2048, 2048], P('tp'), may hold values from -0.125 to 0.125
- gate_weight: bfloat16 [2048, 5632], P('sp', 'tp'), may hold values from -0.125 to 0.125
- up_weight: bfloat16 [2048, 5632], P('sp', 'tp'), may hold values from -0.125 to 0.125
- down_weight: bfloat16 [5632, 2048], P('tp', 'sp'), may hold values from -0.078125 to 0.078125
- conv_taps: float32 [3, 5632], P(None, 'tp'), may hold values from -3.5 to 3.5
- norm_gains: float32 [3, 2048], replicated, may hold values from 0.1 to 1.9
Outputs:
- layer_out: bfloat16 [8192, 2048], P(('sp', 'tp'))
All inputs are finite; a program needn't handle non-finite values.
Results may differ from a plain program's by a relative error of at most 0.02.
Values may be sent and summed in bfloat16 or wider, within the bound.
No kernel may reach another device: no remote copies, remote signals or barrier semaphores. Data moves between devices by JAX's collectives and lax.ppermute only.
A program may use at most 128 MiB of HBM per device.

v0:
```python
import jax
import jax.numpy as jnp
from jax import lax
from jax.sharding import PartitionSpec as P

HEAD = 64
WINDOW = 128
rope_base = 10000.0
neg_large = -1e30
norm_eps = 1e-06


def padded(cells, sides, width):
    for axis, dim in sides:
        count = lax.axis_size(axis)
        ends = count - 1
        head = lax.slice_in_dim(cells, 0, width, axis=dim)
        tail = lax.slice_in_dim(cells, cells.shape[dim] - width, cells.shape[dim], axis=dim)
        cells = jnp.concatenate(
            [
                lax.ppermute(tail, axis, [(i, (i + 1) % count) for i in range(ends)]),
                cells,
                lax.ppermute(head, axis, [((i + 1) % count, i) for i in range(ends)]),
            ],
            axis=dim,
        )
    return cells


def rotate(block, positions):
    rows = block.shape[0]
    heads = block.shape[1] // HEAD
    half = HEAD // 2
    freq = rope_base ** (-jnp.arange(half, dtype=jnp.float32) * 2.0 / HEAD)
    angle = positions.astype(jnp.float32)[:, None] * freq[None, :]
    cosine = jnp.cos(angle)[:, None, :]
    sine = jnp.sin(angle)[:, None, :]
    shaped = block.astype(jnp.float32).reshape(rows, heads, 2, half)
    first = shaped[:, :, 0]
    second = shaped[:, :, 1]
    turned = jnp.stack([first * cosine - second * sine, second * cosine + first * sine], axis=2)
    return turned.reshape(rows, heads * HEAD).astype(jnp.bfloat16)


def attend(queries, keys, values, allowed, sink):
    rows = queries.shape[0]
    kv_local = keys.shape[1] // HEAD
    group = queries.shape[1] // HEAD // kv_local
    shaped_q = queries.reshape(rows, kv_local, group, HEAD)
    shaped_k = keys.reshape(keys.shape[0], kv_local, HEAD)
    shaped_v = values.reshape(values.shape[0], kv_local, HEAD)
    scores = jnp.einsum(
        "qngd,knd->ngqk", shaped_q, shaped_k, preferred_element_type=jnp.float32
    ) * HEAD ** (-0.5)
    scores = jnp.where(allowed[None, None], scores, neg_large)
    sink_group = sink.reshape(kv_local, group)[:, :, None]
    top = jnp.maximum(jnp.max(scores, axis=-1), sink_group)
    weights = jnp.exp(scores - top[..., None])
    total = jnp.sum(weights, axis=-1) + jnp.exp(sink_group - top)
    probs = (weights / total[..., None]).astype(jnp.bfloat16)
    out = jnp.einsum("ngqk,knd->qngd", probs, shaped_v, preferred_element_type=jnp.float32)
    return out.reshape(rows, kv_local * group * HEAD).astype(jnp.bfloat16)


def normalize(vector, gain):
    scale = lax.rsqrt(jnp.mean(vector * vector, axis=-1, keepdims=True) + norm_eps)
    return vector * scale * gain


def local(
    residual_in,
    queries,
    keys,
    values,
    docs,
    sink,
    out_weight,
    gate_weight,
    up_weight,
    down_weight,
    conv_taps,
    norm_gains,
):
    rows = queries.shape[0]
    offset = lax.axis_index("sp") * rows
    total_len = lax.axis_size("sp") * rows
    keys_ext, values_ext, docs_ext = (
        padded(keys, (("sp", 0),), WINDOW),
        padded(values, (("sp", 0),), WINDOW),
        padded(docs, (("sp", 0),), WINDOW),
    )
    here = offset + jnp.arange(rows, dtype=jnp.int32)
    there = offset - WINDOW + jnp.arange(rows + 2 * WINDOW, dtype=jnp.int32)
    q_rot = rotate(queries, here)
    k_rot = rotate(keys_ext, there)
    allowed = (
        (jnp.abs(there[None, :] - here[:, None]) <= WINDOW)
        & (there[None, :] >= 0)
        & (there[None, :] < total_len)
        & (docs_ext[None, :] == docs[:, None])
    )
    attended = attend(q_rot, k_rot, values_ext, allowed, sink)
    mixed = lax.psum_scatter(
        jnp.dot(attended, out_weight, preferred_element_type=jnp.float32).astype(jnp.bfloat16),
        "tp",
        scatter_dimension=0,
        tiled=True,
    ).astype(jnp.float32)
    updated = (residual_in.astype(jnp.float32) + normalize(mixed, norm_gains[0])).astype(
        jnp.bfloat16
    )
    normed = normalize(updated.astype(jnp.float32), norm_gains[1]).astype(jnp.bfloat16)
    ffn_in = lax.all_gather(normed, "tp", axis=0, tiled=True)
    gate = jnp.dot(
        ffn_in,
        lax.all_gather(gate_weight, "sp", axis=0, tiled=True),
        preferred_element_type=jnp.float32,
    )
    up = jnp.dot(
        ffn_in,
        lax.all_gather(up_weight, "sp", axis=0, tiled=True),
        preferred_element_type=jnp.float32,
    )
    gate_low = gate.astype(jnp.bfloat16)
    gate_ext = padded(gate_low, (("sp", 0),), 1).astype(jnp.float32)
    same_prev = (docs_ext[WINDOW - 1 : WINDOW - 1 + rows] == docs)[:, None]
    same_next = (docs_ext[WINDOW + 1 : WINDOW + 1 + rows] == docs)[:, None]
    conv = (
        conv_taps[0] * jnp.where(same_prev, gate_ext[:-2], 0.0)
        + conv_taps[1] * gate_ext[1:-1]
        + conv_taps[2] * jnp.where(same_next, gate_ext[2:], 0.0)
    )
    hidden = (jax.nn.silu(conv) * up).astype(jnp.bfloat16)
    terms = jnp.dot(
        hidden,
        lax.all_gather(down_weight, "sp", axis=1, tiled=True),
        preferred_element_type=jnp.float32,
    )
    ffn_out = lax.psum_scatter(
        terms.astype(jnp.bfloat16), "tp", scatter_dimension=0, tiled=True
    ).astype(jnp.float32)
    return (updated.astype(jnp.float32) + normalize(ffn_out, norm_gains[2])).astype(jnp.bfloat16)


def solution(mesh):
    in_specs = (
        P(("sp", "tp"), None),
        P("sp", "tp"),
        P("sp", "tp"),
        P("sp", "tp"),
        P("sp"),
        P("tp"),
        P("tp", None),
        P("sp", "tp"),
        P("sp", "tp"),
        P("tp", "sp"),
        P(None, "tp"),
        P(),
    )
    out_specs = P(("sp", "tp"), None)
    return jax.shard_map(local, mesh=mesh, in_specs=in_specs, out_specs=out_specs, check_vma=False)
```

profile of v0, /device:TPU:0, one launch (start us, length us, event | category | flops | bytes accessed | tf_op | source)
XLA Modules:
  0.0 611.7 jit_solution(4927613826209139854)
XLA Ops:
  6.5 1.1 copy.21
  7.6 0.0 copy-start.6
  7.6 0.0 copy-start.3
  7.7 4.9 collective-permute-start.4
  12.6 1.3 collective-permute-start.5
  13.9 0.8 fusion.38
  14.6 4.5 collective-permute-start.2
  19.2 1.3 collective-permute-start.3
  20.5 1.5 fusion.36
  22.0 4.9 collective-permute-start
  27.0 0.4 multiply_cosine_fusion
  27.4 0.3 multiply_cosine_fusion.1
  27.7 1.5 copy.24
  29.2 0.3 convert.17
  29.5 0.4 subtract_convert_fusion
  29.9 1.1 pad_maximum_fusion
  31.0 0.1 max.17
  31.0 1.3 collective-permute-start.1
  32.4 1.0 fusion.23
  33.4 0.1 maximum_convert_fusion.1
  33.5 0.1 subtract_convert_fusion.1
  33.6 0.8 pad_maximum_fusion.2
  34.4 5.1 fusion.1
  39.5 0.1 broadcast_maximum_fusion
  39.6 5.3 fusion
  44.9 3.0 copy-done
  47.9 0.7 exponential_add_fusion
  48.7 0.2 copy.20
  48.8 0.0 copy-start.7
  48.8 12.0 %fusion.24 = bf16[4,64,4,512]{3,1,2,0:T(8,128)(2,1)S(1)} fusion(bf16[768,4,64,1]{0,2,3,1:T(8,128)(2,1)S(1)} %bitcast.47, f32[4,768,512,4]{2,1,3,0:T(8,128)} %copy-done, f32[4,4,512]{2,1,0:T(4,128)} %exponential_add_fusion, f32[4,4,512]{2,1,0:T(4,128)S(1)} %broadcast_maximum_fusion, pred[512,768]{0,1:T(8,128)(4,1)S(1)} %fusion.23), kind=kOutput, calls=%fused_computation.42 | convolution fusion | flops 837287936 | bytes 27066368 | tf_op jit(solution)/shard_map/ngqk,knd->qngd/dot_general | solution.py:61
  60.9 0.0 copy-start.5
  60.9 0.0 copy-start.1
  60.9 3.8 convolution_convert_fusion.1
  64.7 0.0 reduce-scatter.3.cloned.1.call-update
  64.7 0.0 all-gather.5.cloned.1.call-start
  64.8 15.3 %reduce-scatter.3.cloned.1.call-done = bf16[256,2048]{1,0:T(8,128)(2,1)} async-done(((bf16[512,2048]{1,0:T(8,128)(2,1)}), bf16[256,2048]{1,0:T(8,128)(2,1)}) %reduce-scatter.3.cloned.1.call-update) | async-done | bytes 1048592 | tf_op jit(solution)/shard_map/reduce_scatter | solution.py:103
  80.1 1.5 fusion.11
  81.7 1.9 fusion.17
  83.6 1.3 fusion.19
  84.8 0.0 all-gather.5.cloned.1.call-update
  84.9 0.0 all-gather.7.cloned.1.call-start
  84.9 0.7 all-gather.7.cloned.1.call-update
  85.6 0.0 all-gather.11.cloned.1.call-start
  85.7 0.5 all-gather.11.cloned.1.call-update
  86.2 0.0 all-gather.9.cloned.1.call-start
  86.2 0.5 all-gather.9.cloned.1.call-update
  86.8 0.2 reduce-scatter.5.cloned.1.call-start
  87.0 0.1 slice_reduce_fusion.2
  87.1 9.8 %all-gather.5.cloned.1.call-done = bf16[512,2048]{1,0:T(8,128)(2,1)} async-done(((bf16[256,2048]{1,0:T(8,128)(2,1)}), bf16[512,2048]{1,0:T(8,128)(2,1)}) %all-gather.5.cloned.1.call-update) | async-done | bytes 2097168 | tf_op jit(solution)/shard_map/all_gather | solution.py:113
  96.9 145.4 %all-gather.7.cloned.1.call-done = bf16[2048,2816]{1,0:T(8,128)(2,1)} async-done(((bf16[128,2816]{1,0:T(8,128)(2,1)}), bf16[2048,2816]{1,0:T(8,128)(2,1)}) %all-gather.7.cloned.1.call-update) | async-done | bytes 11534352 | tf_op jit(solution)/shard_map/all_gather | solution.py:116
  242.3 10.9 %convolution_convert_fusion = bf16[512,2816]{1,0:T(8,128)(2,1)S(1)} fusion(bf16[512,2048]{1,0:T(8,128)(2,1)} %all-gather.5.cloned.1.call-done, bf16[2048,2816]{1,0:T(8,128)(2,1)} %all-gather.7.cloned.1.call-done), kind=kOutput, calls=%fused_computation.14 | convolution fusion | flops 5907021824 | bytes 16515072 | tf_op jit(solution)/shard_map/dot_general | solution.py:114
  253.3 3.2 collective-permute-start.6
  256.4 1.3 collective-permute-start.7
  257.7 0.1 slice_compare_fusion.1
  257.8 0.2 collective-permute-done.6
  258.0 4.4 collective-permute-done.7
  262.4 3.1 maximum_convert_fusion
  265.5 159.9 %all-gather.11.cloned.1.call-done = bf16[2816,2048]{1,0:T(8,128)(2,1)} async-done(((bf16[2816,128]{1,0:T(8,128)(2,1)}), bf16[2816,2048]{1,0:T(8,128)(2,1)}) %all-gather.11.cloned.1.call-update) | async-done | bytes 11534352 | tf_op jit(solution)/shard_map/all_gather | solution.py:136
  425.3 142.2 %all-gather.9.cloned.1.call-done = bf16[2048,2816]{1,0:T(8,128)(2,1)} async-done(((bf16[128,2816]{1,0:T(8,128)(2,1)}), bf16[2048,2816]{1,0:T(8,128)(2,1)}) %all-gather.9.cloned.1.call-update) | async-done | bytes 11534352 | tf_op jit(solution)/shard_map/all_gather | solution.py:121
  567.6 25.0 %convolution_convert_fusion.2 = bf16[512,2048]{1,0:T(8,128)(2,1)} fusion(bf16[2816,2048]{1,0:T(8,128)(2,1)} %all-gather.11.cloned.1.call-done, f32[514,2816]{1,0:T(8,128)} %maximum_convert_fusion, f32[2816]{0:T(1024)S(1)} %get-tuple-element.6, f32[2816]{0:T(1024)S(1)} %get-tuple-element.7, f32[2816]{0:T(1024)S(1)} %get-tuple-element.5, ...), kind=kOutput, calls=%fused_computation.19 | convolution fusion | flops 11830951936 | bytes 44599296 | tf_op jit(solution)/shard_map/dot_general | solution.py:134
  592.6 0.0 reduce-scatter.5.cloned.1.call-update
  592.6 8.1 %reduce-scatter.5.cloned.1.call-done = bf16[256,2048]{1,0:T(8,128)(2,1)} async-done(((bf16[512,2048]{1,0:T(8,128)(2,1)}), bf16[256,2048]{1,0:T(8,128)(2,1)}) %reduce-scatter.5.cloned.1.call-update) | async-done | bytes 1048592 | tf_op jit(solution)/shard_map/reduce_scatter | solution.py:139
  600.7 1.5 fusion.15
  602.2 2.6 fusion.20
  (32 shorter events, 0.2 us)
Async XLA Ops:
  6.5 73.6 %reduce-scatter.3.cloned.1.call-start = ((), (), s32[]{:S(2)}) async-start(), calls=%async_computation.2 | async-start | bytes 3145728 | tf_op jit(solution)/shard_map/reduce_scatter | solution.py:103
  7.6 23.3 %copy-start.6 = (f32[16]{0:T(128)S(1)}, f32[16]{0:T(128)}, u32[]{:S(2)}) copy-start(f32[16]{0:T(128)} %param.17) | copy-start | bytes 196
  7.6 24.7 %copy-start.3 = (s32[512]{0:T(512)S(1)}, s32[512]{0:T(512)}, u32[]{:S(2)}) copy-start(s32[512]{0:T(512)} %param.16) | copy-start | bytes 6148
  7.7 25.7 %collective-permute-start.4 = (bf16[128,256]{0,1:T(8,128)(2,1)S(1)}, bf16[128,256]{0,1:T(8,128)(2,1)S(1)}, u32[]{:S(2)}, u32[]{:S(2)}) collective-permute-start(bf16[128,256]{0,1:T(8,128)(2,1)S(1)} %get-tuple-element.16), channel_id=1, source_target_pairs={{0,2},{2,4},{4,6},{6,8},{8,10},{10,12},{12,14},{14,16},{16,18},{18... | collective-permute-start | bytes 196616 | tf_op jit(solution)/shard_map/ppermute | solution.py:21
  12.6 20.9 %collective-permute-start.5 = (bf16[128,256]{0,1:T(8,128)(2,1)S(1)}, bf16[128,256]{0,1:T(8,128)(2,1)S(1)}, u32[]{:S(2)}, u32[]{:S(2)}) collective-permute-start(bf16[128,256]{0,1:T(8,128)(2,1)S(1)} %get-tuple-element.17), channel_id=1, source_target_pairs={{2,0},{4,2},{6,4},{8,6},{10,8},{12,10},{14,12},{16,14},{18,16},{20... | collective-permute-start | bytes 196616 | tf_op jit(solution)/shard_map/ppermute | solution.py:23
  14.6 16.4 %collective-permute-start.2 = (s32[128]{0:T(128)S(1)}, s32[128]{0:T(128)S(1)}, u32[]{:S(2)}, u32[]{:S(2)}) collective-permute-start(s32[128]{0:T(128)S(1)} %get-tuple-element.31), channel_id=1, source_target_pairs={{0,2},{2,4},{4,6},{6,8},{8,10},{10,12},{12,14},{14,16},{16,18},{18... | collective-permute-start | bytes 1544 | tf_op jit(solution)/shard_map/ppermute | solution.py:21
  19.2 13.2 %collective-permute-start.3 = (s32[128]{0:T(128)S(1)}, s32[128]{0:T(128)S(1)}, u32[]{:S(2)}, u32[]{:S(2)}) collective-permute-start(s32[128]{0:T(128)S(1)} %get-tuple-element.32), channel_id=1, source_target_pairs={{2,0},{4,2},{6,4},{8,6},{10,8},{12,10},{14,12},{16,14},{18,16},{20... | collective-permute-start | bytes 1544 | tf_op jit(solution)/shard_map/ppermute | solution.py:23
  22.0 26.6 %collective-permute-start = (bf16[128,256]{1,0:T(8,128)(2,1)}, bf16[128,256]{1,0:T(8,128)(2,1)S(1)}, u32[]{:S(2)}, u32[]{:S(2)}) collective-permute-start(bf16[128,256]{1,0:T(8,128)(2,1)} %get-tuple-element.18), channel_id=1, source_target_pairs={{0,2},{2,4},{4,6},{6,8},{8,10},{10,12},{12,14},{14,16},{16,18},{18... | collective-permute-start | bytes 196616 | tf_op jit(solution)/shard_map/ppermute | solution.py:21
  31.0 17.6 %collective-permute-start.1 = (bf16[128,256]{1,0:T(8,128)(2,1)}, bf16[128,256]{1,0:T(8,128)(2,1)S(1)}, u32[]{:S(2)}, u32[]{:S(2)}) collective-permute-start(bf16[128,256]{1,0:T(8,128)(2,1)} %get-tuple-element.19), channel_id=1, source_target_pairs={{2,0},{4,2},{6,4},{8,6},{10,8},{12,10},{14,12},{16,14},{18,16},{20... | collective-permute-start | bytes 196616 | tf_op jit(solution)/shard_map/ppermute | solution.py:23
  39.5 8.4 %copy-start = (f32[4,768,512,4]{2,1,3,0:T(8,128)}, f32[4,768,512,4]{2,1,3,0:T(8,128)S(1)}, u32[]{:S(2)}) copy-start(f32[4,768,512,4]{2,1,3,0:T(8,128)S(1)} %get-tuple-element.34) | copy-start | bytes 75497472
  39.6 9.0 %copy-start.2 = (bf16[512,256]{1,0:T(8,128)(2,1)S(1)}, bf16[512,256]{1,0:T(8,128)(2,1)}, u32[]{:S(2)}) copy-start(bf16[512,256]{1,0:T(8,128)(2,1)} %param.15) | copy-start | bytes 786436
  48.8 12.0 %copy-start.7 = (bf16[1024,2048]{1,0:T(8,128)(2,1)S(1)}, bf16[1024,2048]{1,0:T(8,128)(2,1)}, u32[]{:S(2)}) copy-start(bf16[1024,2048]{1,0:T(8,128)(2,1)} %param.18) | copy-start | bytes 12582916
  60.9 3.9 copy-start.5
  60.9 20.8 %copy-start.1 = (bf16[256,2048]{1,0:T(8,128)(2,1)S(1)}, bf16[256,2048]{1,0:T(8,128)(2,1)}, u32[]{:S(2)}) copy-start(bf16[256,2048]{1,0:T(8,128)(2,1)} %param.12) | copy-start | bytes 3145732
  64.7 22.3 %copy-start.4 = (f32[3,2816]{1,0:T(4,128)S(1)}, f32[3,2816]{1,0:T(4,128)}, u32[]{:S(2)}) copy-start(f32[3,2816]{1,0:T(4,128)} %param.22) | copy-start | bytes 101380
  64.7 32.2 %all-gather.5.cloned.1.call-start = ((), (), s32[]{:S(2)}) async-start(), calls=%async_computation.3 | async-start | bytes 3145728 | tf_op jit(solution)/shard_map/all_gather | solution.py:113
  84.9 157.4 %all-gather.7.cloned.1.call-start = ((), (), s32[]{:S(2)}) async-start(), calls=%async_computation.4 | async-start | bytes 12255232 | tf_op jit(solution)/shard_map/all_gather | solution.py:116
  85.6 339.7 %all-gather.11.cloned.1.call-start = ((), (), s32[]{:S(2)}) async-start(), calls=%async_computation.6 | async-start | bytes 12255232 | tf_op jit(solution)/shard_map/all_gather | solution.py:136
  86.2 481.4 %all-gather.9.cloned.1.call-start = ((), (), s32[]{:S(2)}) async-start(), calls=%async_computation.5 | async-start | bytes 12255232 | tf_op jit(solution)/shard_map/all_gather | solution.py:121
  86.8 513.9 %reduce-scatter.5.cloned.1.call-start = ((), (), s32[]{:S(2)}) async-start(), calls=%async_computation.7 | async-start | bytes 3145728 | tf_op jit(solution)/shard_map/reduce_scatter | solution.py:139
  253.3 4.7 collective-permute-start.6
  256.4 5.9 collective-permute-start.7
Sparse Core Ops, SparseCore 0:
  64.8 15.2 reduce-scatter.2
  85.0 11.8 all-gather.4
  99.7 142.5 all-gather.6
  244.8 180.4 all-gather.10
  427.9 139.5 all-gather.8
  592.7 7.9 reduce-scatter.4
where the time goes:
time: 612 us
  waiting for transfers between devices  487 us (80%)
  matrix products  56.8 us (9%)
  starting transfers between devices  23 us (4%)
  other arithmetic  22.6 us (4%)
  between operations  13.9 us (2%)
  local copies, waits for them, and re-layouts  8.33 us (1%)
    all_gather x1, waiting for transfers between devices, local(): lax.all_gather(down_weight, 'sp', axis=1, tiled=True)  160 us
    all_gather x1, waiting for transfers between devices, local(): lax.all_gather(gate_weight, 'sp', axis=0, tiled=True)  145 us
    all_gather x1, waiting for transfers between devices, local(): lax.all_gather(up_weight, 'sp', axis=0, tiled=True)  142 us
    dot_general x1, matrix products, local(): jnp.dot(hidden, lax.all_gather(down_weight, 'sp', axis=1, tiled=True), pr...  25 us
    ppermute x4, starting transfers between devices, padded(): lax.ppermute(tail, axis, [(i, (i + 1) % count) for i in range(ends)])  17.5 us
    reduce_scatter x1, waiting for transfers between devices, local(): lax.psum_scatter(jnp.dot(attended, out_weight, preferred_element_type=jnp...  15.3 us
  transfers between devices with their start and end apart: 14, of which 8 were waited for; matrix products, arithmetic and copies ran while one was open for 6% of the time, Pallas kernels for 0%

commit v1 on v0

--- a/solution.py
+++ b/solution.py
@@ -131,11 +131,11 @@
         + conv_taps[2] * jnp.where(same_next, gate_ext[2:], 0.0)
     )
     hidden = (jax.nn.silu(conv) * up).astype(jnp.bfloat16)
-    terms = jnp.dot(
-        hidden,
-        lax.all_gather(down_weight, "sp", axis=1, tiled=True),
-        preferred_element_type=jnp.float32,
-    )
+
+    def end_waves(chunk, axis_tag):
+        return jnp.concatenate(lax.all_gather(chunk, axis_tag), 1)
+
+    terms = jnp.dot(hidden, end_waves(down_weight, "sp"), preferred_element_type=jnp.float32)
     ffn_out = lax.psum_scatter(
         terms.astype(jnp.bfloat16), "tp", scatter_dimension=0, tiled=True
     ).astype(jnp.float32)

time: 612 us -> 571 us (0.933)
  waiting for transfers between devices: 487 us -> 428 us
  local copies, waits for them, and re-layouts: 8.33 us -> 25.2 us
    all_gather x1, waiting for transfers between devices: 160 us -> 125 us  [end_waves(): return jnp.concatenate(lax.all_gather(chunk, axis_tag), 1)]
    all_gather x1, waiting for transfers between devices: 142 us -> 122 us  [local(): lax.all_gather(up_weight, 'sp', axis=0, tiled=True)]
    reshape x0 -> x1, local copies, waits for them, and re-layouts: none -> 15.2 us  [end_waves(): return jnp.concatenate(lax.all_gather(chunk, axis_tag), 1)]
  transfers between devices with their start and end apart: 14 -> 14, of which waited for: 8 -> 6; matrix products, arithmetic and copies ran while one was open for 6% -> 9% of each run, Pallas kernels for 0% -> 0%
where the time goes in v1:
time: 571 us; the launch traced here: 570 us
  waiting for transfers between devices  428 us (75%)
  matrix products  56.2 us (10%)
  local copies, waits for them, and re-layouts  25.2 us (4%)
  other arithmetic  24.4 us (4%)
  starting transfers between devices  23 us (4%)
  between operations  13.9 us (2%)
    all_gather x1, waiting for transfers between devices, local(): lax.all_gather(gate_weight, 'sp', axis=0, tiled=True)  145 us
    all_gather x1, waiting for transfers between devices, end_waves(): return jnp.concatenate(lax.all_gather(chunk, axis_tag), 1)  125 us
    all_gather x1, waiting for transfers between devices, local(): lax.all_gather(up_weight, 'sp', axis=0, tiled=True)  122 us
    dot_general x1, matrix products, local(): jnp.dot(hidden, end_waves(down_weight, 'sp'), preferred_element_type=jnp....  24.3 us
    ppermute x4, starting transfers between devices, padded(): lax.ppermute(tail, axis, [(i, (i + 1) % count) for i in range(ends)])  17.5 us
    reduce_scatter x1, waiting for transfers between devices, local(): lax.psum_scatter(jnp.dot(attended, out_weight, preferred_element_type=jnp...  15.3 us
    reshape x1, local copies, waits for them, and re-layouts, end_waves(): return jnp.concatenate(lax.all_gather(chunk, axis_tag), 1)  15.2 us
    dot_general x1, matrix products, attend(): jnp.einsum('ngqk,knd->qngd', probs, shaped_v, preferred_element_type=jnp....  12 us
  transfers between devices with their start and end apart: 14, of which 6 were waited for; matrix products, arithmetic and copies ran while one was open for 9% of the time, Pallas kernels for 0%

profile of v1, /device:TPU:0, one launch (start us, length us, event | category | flops | bytes accessed | tf_op | source)
XLA Modules:
  0.0 570.5 jit_solution(5342564187769399239)
XLA Ops:
  6.5 1.1 copy.27
  7.6 0.0 copy-start.7
  7.6 0.0 copy-start.4
  7.7 4.9 collective-permute-start.4
  12.6 1.3 collective-permute-start.5
  13.9 0.8 fusion.38
  14.6 4.5 collective-permute-start.2
  19.2 1.3 collective-permute-start.3
  20.5 1.5 fusion.36
  22.0 4.9 collective-permute-start
  27.0 0.4 multiply_cosine_fusion
  27.4 0.3 multiply_cosine_fusion.1
  27.7 1.5 copy.30
  29.2 0.3 convert.17
  29.5 0.4 subtract_convert_fusion
  29.9 1.1 pad_maximum_fusion
  31.0 0.1 max.17
  31.1 1.3 collective-permute-start.1
  32.4 1.0 fusion.23
  33.4 0.1 maximum_convert_fusion.1
  33.5 0.1 subtract_convert_fusion.1
  33.6 0.8 pad_maximum_fusion.2
  34.4 5.1 fusion.1
  39.5 0.1 broadcast_maximum_fusion
  39.6 5.3 fusion
  44.9 3.0 copy-done
  47.9 0.7 exponential_add_fusion
  48.7 0.2 copy.26
  48.9 0.0 copy-start.8
  48.9 12.0 %fusion.24 = bf16[4,64,4,512]{3,1,2,0:T(8,128)(2,1)S(1)} fusion(bf16[768,4,64,1]{0,2,3,1:T(8,128)(2,1)S(1)} %bitcast.53, f32[4,768,512,4]{2,1,3,0:T(8,128)} %copy-done, f32[4,4,512]{2,1,0:T(4,128)} %exponential_add_fusion, f32[4,4,512]{2,1,0:T(4,128)S(1)} %broadcast_maximum_fusion, pred[512,768]{0,1:T(8,128)(4,1)S(1)} %fusion.23), kind=kOutput, calls=%fused_computation.42 | convolution fusion | flops 837287936 | bytes 27066368 | tf_op jit(solution)/shard_map/ngqk,knd->qngd/dot_general | solution.py:61
  60.9 0.0 copy-start.6
  60.9 0.0 copy-start.2
  60.9 3.8 convolution_convert_fusion.1
  64.7 0.0 reduce-scatter.3.cloned.1.call-update
  64.7 0.0 all-gather.6.cloned.1.call-start
  64.8 15.3 %reduce-scatter.3.cloned.1.call-done = bf16[256,2048]{1,0:T(8,128)(2,1)} async-done(((bf16[512,2048]{1,0:T(8,128)(2,1)}), bf16[256,2048]{1,0:T(8,128)(2,1)}) %reduce-scatter.3.cloned.1.call-update) | async-done | bytes 1048592 | tf_op jit(solution)/shard_map/reduce_scatter | solution.py:103
  80.2 1.5 fusion.11
  81.7 1.9 fusion.17
  83.6 1.3 fusion.19
  84.9 0.0 all-gather.6.cloned.1.call-update
  84.9 0.0 all-gather.8.cloned.1.call-start
  84.9 0.7 all-gather.8.cloned.1.call-update
  85.6 0.0 all-gather.12.cloned.1.call-start
  85.7 0.5 all-gather.12.cloned.1.call-update
  86.2 0.0 all-gather.10.cloned.1.call-start
  86.2 0.5 all-gather.10.cloned.1.call-update
  86.8 0.2 reduce-scatter.5.cloned.1.call-start
  87.0 0.1 slice_reduce_fusion.2
  87.1 9.8 %all-gather.6.cloned.1.call-done = bf16[512,2048]{1,0:T(8,128)(2,1)} async-done(((bf16[256,2048]{1,0:T(8,128)(2,1)}), bf16[512,2048]{1,0:T(8,128)(2,1)}) %all-gather.6.cloned.1.call-update) | async-done | bytes 2097168 | tf_op jit(solution)/shard_map/all_gather | solution.py:113
  96.9 145.4 %all-gather.8.cloned.1.call-done = bf16[2048,2816]{1,0:T(8,128)(2,1)} async-done(((bf16[128,2816]{1,0:T(8,128)(2,1)}), bf16[2048,2816]{1,0:T(8,128)(2,1)}) %all-gather.8.cloned.1.call-update) | async-done | bytes 11534352 | tf_op jit(solution)/shard_map/all_gather | solution.py:116
  242.3 10.9 %convolution_convert_fusion = bf16[512,2816]{1,0:T(8,128)(2,1)S(1)} fusion(bf16[512,2048]{1,0:T(8,128)(2,1)} %all-gather.6.cloned.1.call-done, bf16[2048,2816]{1,0:T(8,128)(2,1)} %all-gather.8.cloned.1.call-done), kind=kOutput, calls=%fused_computation.14 | convolution fusion | flops 5907021824 | bytes 16515072 | tf_op jit(solution)/shard_map/dot_general | solution.py:114
  253.3 1.6 copy-done.1
  254.9 3.2 collective-permute-start.6
  258.1 1.3 collective-permute-start.7
  259.4 0.1 slice_compare_fusion.1
  259.5 125.3 %all-gather.12.cloned.1.call-done = bf16[45056,128]{1,0:T(8,128)(2,1)} async-done(((bf16[2816,128]{1,0:T(8,128)(2,1)}), bf16[45056,128]{1,0:T(8,128)(2,1)}) %all-gather.12.cloned.1.call-update) | async-done | bytes 11534352 | tf_op jit(solution)/shard_map/all_gather | solution.py:136
  384.8 15.2 %copy.32 = bf16[2816,16,128]{0,2,1:T(8,128)(2,1)} copy(bf16[2816,16,128]{2,0,1:T(8,128)(2,1)} %bitcast.47) | data formatting | bytes 23068672 | tf_op jit(solution)/shard_map/reshape | solution.py:136
  400.0 5.0 maximum_convert_fusion
  404.9 122.1 %all-gather.10.cloned.1.call-done = bf16[2048,2816]{1,0:T(8,128)(2,1)} async-done(((bf16[128,2816]{1,0:T(8,128)(2,1)}), bf16[2048,2816]{1,0:T(8,128)(2,1)}) %all-gather.10.cloned.1.call-update) | async-done | bytes 11534352 | tf_op jit(solution)/shard_map/all_gather | solution.py:121
  527.0 24.3 %convolution_convert_fusion.2 = bf16[512,2048]{1,0:T(8,128)(2,1)} fusion(bf16[2816,2048]{0,1:T(8,128)(2,1)} %bitcast.48, f32[514,2816]{1,0:T(8,128)} %maximum_convert_fusion, f32[2816]{0:T(1024)S(1)} %get-tuple-element.6, f32[2816]{0:T(1024)S(1)} %get-tuple-element.7, f32[2816]{0:T(1024)S(1)} %get-tuple-element.5, pred[512]{0:T(512)(128)(4,1)S(1)} %get-tuple-element.28, ...), kind=kOutput, calls=%fused_computation.19 | convolution fusion | flops 11830951936 | bytes 44599296 | tf_op jit(solution)/shard_map/dot_general | solution.py:138
  551.3 0.0 reduce-scatter.5.cloned.1.call-update
  551.4 8.1 %reduce-scatter.5.cloned.1.call-done = bf16[256,2048]{1,0:T(8,128)(2,1)} async-done(((bf16[512,2048]{1,0:T(8,128)(2,1)}), bf16[256,2048]{1,0:T(8,128)(2,1)}) %reduce-scatter.5.cloned.1.call-update) | async-done | bytes 1048592 | tf_op jit(solution)/shard_map/reduce_scatter | solution.py:139
  559.4 1.5 fusion.15
  561.0 2.6 fusion.20
  (35 shorter events, 0.2 us)
Async XLA Ops:
  6.5 73.6 %reduce-scatter.3.cloned.1.call-start = ((), (), s32[]{:S(2)}) async-start(), calls=%async_computation.2 | async-start | bytes 3145728 | tf_op jit(solution)/shard_map/reduce_scatter | solution.py:103
  7.6 23.3 %copy-start.7 = (f32[16]{0:T(128)S(1)}, f32[16]{0:T(128)}, u32[]{:S(2)}) copy-start(f32[16]{0:T(128)} %param.17) | copy-start | bytes 196
  7.6 24.7 %copy-start.4 = (s32[512]{0:T(512)S(1)}, s32[512]{0:T(512)}, u32[]{:S(2)}) copy-start(s32[512]{0:T(512)} %param.16) | copy-start | bytes 6148
  7.7 25.7 %collective-permute-start.4 = (bf16[128,256]{0,1:T(8,128)(2,1)S(1)}, bf16[128,256]{0,1:T(8,128)(2,1)S(1)}, u32[]{:S(2)}, u32[]{:S(2)}) collective-permute-start(bf16[128,256]{0,1:T(8,128)(2,1)S(1)} %get-tuple-element.16), channel_id=1, source_target_pairs={{0,2},{2,4},{4,6},{6,8},{8,10},{10,12},{12,14},{14,16},{16,18},{18... | collective-permute-start | bytes 196616 | tf_op jit(solution)/shard_map/ppermute | solution.py:21
  12.6 20.9 %collective-permute-start.5 = (bf16[128,256]{0,1:T(8,128)(2,1)S(1)}, bf16[128,256]{0,1:T(8,128)(2,1)S(1)}, u32[]{:S(2)}, u32[]{:S(2)}) collective-permute-start(bf16[128,256]{0,1:T(8,128)(2,1)S(1)} %get-tuple-element.17), channel_id=1, source_target_pairs={{2,0},{4,2},{6,4},{8,6},{10,8},{12,10},{14,12},{16,14},{18,16},{20... | collective-permute-start | bytes 196616 | tf_op jit(solution)/shard_map/ppermute | solution.py:23
  14.6 16.4 %collective-permute-start.2 = (s32[128]{0:T(128)S(1)}, s32[128]{0:T(128)S(1)}, u32[]{:S(2)}, u32[]{:S(2)}) collective-permute-start(s32[128]{0:T(128)S(1)} %get-tuple-element.31), channel_id=1, source_target_pairs={{0,2},{2,4},{4,6},{6,8},{8,10},{10,12},{12,14},{14,16},{16,18},{18... | collective-permute-start | bytes 1544 | tf_op jit(solution)/shard_map/ppermute | solution.py:21
  19.2 13.2 %collective-permute-start.3 = (s32[128]{0:T(128)S(1)}, s32[128]{0:T(128)S(1)}, u32[]{:S(2)}, u32[]{:S(2)}) collective-permute-start(s32[128]{0:T(128)S(1)} %get-tuple-element.32), channel_id=1, source_target_pairs={{2,0},{4,2},{6,4},{8,6},{10,8},{12,10},{14,12},{16,14},{18,16},{20... | collective-permute-start | bytes 1544 | tf_op jit(solution)/shard_map/ppermute | solution.py:23
  22.0 26.6 %collective-permute-start = (bf16[128,256]{1,0:T(8,128)(2,1)}, bf16[128,256]{1,0:T(8,128)(2,1)S(1)}, u32[]{:S(2)}, u32[]{:S(2)}) collective-permute-start(bf16[128,256]{1,0:T(8,128)(2,1)} %get-tuple-element.18), channel_id=1, source_target_pairs={{0,2},{2,4},{4,6},{6,8},{8,10},{10,12},{12,14},{14,16},{16,18},{18... | collective-permute-start | bytes 196616 | tf_op jit(solution)/shard_map/ppermute | solution.py:21
  31.1 17.6 %collective-permute-start.1 = (bf16[128,256]{1,0:T(8,128)(2,1)}, bf16[128,256]{1,0:T(8,128)(2,1)S(1)}, u32[]{:S(2)}, u32[]{:S(2)}) collective-permute-start(bf16[128,256]{1,0:T(8,128)(2,1)} %get-tuple-element.19), channel_id=1, source_target_pairs={{2,0},{4,2},{6,4},{8,6},{10,8},{12,10},{14,12},{16,14},{18,16},{20... | collective-permute-start | bytes 196616 | tf_op jit(solution)/shard_map/ppermute | solution.py:23
  39.5 8.4 %copy-start = (f32[4,768,512,4]{2,1,3,0:T(8,128)}, f32[4,768,512,4]{2,1,3,0:T(8,128)S(1)}, u32[]{:S(2)}) copy-start(f32[4,768,512,4]{2,1,3,0:T(8,128)S(1)} %get-tuple-element.34) | copy-start | bytes 75497472
  39.6 9.0 %copy-start.3 = (bf16[512,256]{1,0:T(8,128)(2,1)S(1)}, bf16[512,256]{1,0:T(8,128)(2,1)}, u32[]{:S(2)}) copy-start(bf16[512,256]{1,0:T(8,128)(2,1)} %param.15) | copy-start | bytes 786436
  48.9 12.0 %copy-start.8 = (bf16[1024,2048]{1,0:T(8,128)(2,1)S(1)}, bf16[1024,2048]{1,0:T(8,128)(2,1)}, u32[]{:S(2)}) copy-start(bf16[1024,2048]{1,0:T(8,128)(2,1)} %param.18) | copy-start | bytes 12582916
  60.9 3.9 copy-start.6
  60.9 20.8 %copy-start.2 = (bf16[256,2048]{1,0:T(8,128)(2,1)S(1)}, bf16[256,2048]{1,0:T(8,128)(2,1)}, u32[]{:S(2)}) copy-start(bf16[256,2048]{1,0:T(8,128)(2,1)} %param.12) | copy-start | bytes 3145732
  64.7 22.3 %copy-start.5 = (f32[3,2816]{1,0:T(4,128)S(1)}, f32[3,2816]{1,0:T(4,128)}, u32[]{:S(2)}) copy-start(f32[3,2816]{1,0:T(4,128)} %param.22) | copy-start | bytes 101380
  64.7 32.2 %all-gather.6.cloned.1.call-start = ((), (), s32[]{:S(2)}) async-start(), calls=%async_computation.3 | async-start | bytes 3145728 | tf_op jit(solution)/shard_map/all_gather | solution.py:113
  84.9 157.4 %all-gather.8.cloned.1.call-start = ((), (), s32[]{:S(2)}) async-start(), calls=%async_computation.4 | async-start | bytes 12255232 | tf_op jit(solution)/shard_map/all_gather | solution.py:116
  85.6 299.2 %all-gather.12.cloned.1.call-start = ((), (), s32[]{:S(2)}) async-start(), calls=%async_computation.7 | async-start | bytes 12255232 | tf_op jit(solution)/shard_map/all_gather | solution.py:136
  86.2 440.8 %all-gather.10.cloned.1.call-start = ((), (), s32[]{:S(2)}) async-start(), calls=%async_computation.5 | async-start | bytes 12255232 | tf_op jit(solution)/shard_map/all_gather | solution.py:121
  86.8 472.7 %reduce-scatter.5.cloned.1.call-start = ((), (), s32[]{:S(2)}) async-start(), calls=%async_computation.6 | async-start | bytes 3145728 | tf_op jit(solution)/shard_map/reduce_scatter | solution.py:139
  253.2 1.6 copy-start.1
  254.9 145.1 %collective-permute-start.6 = (bf16[1,2816]{1,0:T(2,128)(2,1)S(1)}, bf16[1,2816]{1,0:T(2,128)(2,1)S(1)}, u32[]{:S(2)}, u32[]{:S(2)}) collective-permute-start(bf16[1,2816]{1,0:T(2,128)(2,1)S(1)} %get-tuple-element.10), channel_id=1, source_target_pairs={{0,2},{2,4},{4,6},{6,8},{8,10},{10,12},{12,14},{14,16},{16,18},{18... | collective-permute-start | bytes 16904 | tf_op jit(solution)/shard_map/ppermute | solution.py:21
  258.1 141.9 %collective-permute-start.7 = (bf16[1,2816]{1,0:T(2,128)(2,1)S(1)}, bf16[1,2816]{1,0:T(2,128)(2,1)S(1)}, u32[]{:S(2)}, u32[]{:S(2)}) collective-permute-start(bf16[1,2816]{1,0:T(2,128)(2,1)S(1)} %get-tuple-element.11), channel_id=1, source_target_pairs={{2,0},{4,2},{6,4},{8,6},{10,8},{12,10},{14,12},{16,14},{18,16},{20... | collective-permute-start | bytes 16904 | tf_op jit(solution)/shard_map/ppermute | solution.py:23
Sparse Core Ops, SparseCore 0:
  64.8 15.2 reduce-scatter.2
  85.0 11.8 all-gather.5
  99.7 142.5 all-gather.7
  244.9 139.8 all-gather.11
  387.4 139.5 all-gather.9
  551.5 7.9 reduce-scatter.4
